TPU v7x, 32 devices: a whole 2x2x4 slice. The times are simulated.
32 devices in a mesh: grp: 2 (over y), fs: 4 (over z), tp: 4 (over x, core).
Axes of the slice: x: 2, y: 2, z: 4, core: 2. Of those that a mesh axis runs over, the one named last changes fastest.
Arguments:
- residual_in: bfloat16 [4096, 2048], P(('grp', 'fs', 'tp')), parts along dimension 0, may hold values from -6 to 6
- hidden_first: bfloat16 [4096, 5632], P(('grp', 'fs', 'tp')), parts along dimension 0, may hold values from -6 to 6
- down_weight: bfloat16 [5632, 2048], P('tp', 'fs'), may hold values from -0.078125 to 0.078125
- mixer_out: bfloat16 [4096, 2048], P(('grp', 'fs', 'tp')), parts along dimension 0, may hold values from -6 to 6
- norm_gain: float32 [2, 2048], replicated, may hold values from 0.1 to 1.9
- norm_shift: float32 [2, 2048], replicated, may hold values from -1.5 to 1.5
- gate_weight: bfloat16 [2048, 5632], P('fs', 'tp'), may hold values from -0.125 to 0.125
- up_weight: bfloat16 [2048, 5632], P('fs', 'tp'), may hold values from -0.125 to 0.125
Outputs:
- mixed_state: bfloat16 [4096, 2048], P(('grp', 'fs', 'tp')), parts along dimension 0
- hidden_second: bfloat16 [4096, 5632], P(('grp', 'fs'), 'tp'), parts along dimension 0
There are 2 independent parts, one for each index of `grp`. A program takes and returns all parts, laid end to end along the dimension named above; an argument that names none is the same for every part. Nothing has to cross between parts.
All inputs are finite; a program needn't handle non-finite values.
Results may differ from a plain program's by a relative error of at most 0.012.
Values may be sent and summed in bfloat16 or wider, within the bound.
A program may use at most 64 MiB of HBM per device.

v0:
```python
import jax
import jax.numpy as jnp
from jax import lax
from jax.sharding import PartitionSpec as P


def layer_norm(values, gain, shift):
    center = values - jnp.mean(values, axis=-1, keepdims=True)
    variance = jnp.mean(center * center, axis=-1, keepdims=True)
    return center * lax.rsqrt(variance + 1e-05) * gain + shift


def on_device(
    residual_in, hidden_first, down_weight, mixer_out, norm_gain, norm_shift, gate_weight, up_weight
):
    spread = lax.all_to_all(hidden_first, "tp", split_axis=1, concat_axis=0, tiled=True)
    down_full = lax.all_gather(down_weight, "fs", axis=1, tiled=True)
    branch = lax.psum_scatter(
        jnp.dot(spread, down_full, preferred_element_type=jnp.float32).astype(jnp.bfloat16),
        "tp",
        scatter_dimension=0,
        tiled=True,
    ).astype(jnp.float32)
    first = layer_norm(
        jnp.sqrt(2.0) * residual_in.astype(jnp.float32) + 0.5 * branch, norm_gain[0], norm_shift[0]
    )
    mixed_state = layer_norm(
        jnp.sqrt(2.0) * first + mixer_out.astype(jnp.float32), norm_gain[1], norm_shift[1]
    ).astype(jnp.bfloat16)
    gathered = lax.all_gather(mixed_state, "tp", axis=0, tiled=True)
    width = gate_weight.shape[1]
    joined = jnp.concatenate([gate_weight, up_weight], axis=1)
    both = jnp.dot(
        gathered,
        lax.all_gather(joined, "fs", axis=0, tiled=True),
        preferred_element_type=jnp.float32,
    )
    gate = both[:, :width]
    up = both[:, width:]
    hidden_second = (jax.nn.silu(gate) * up).astype(jnp.bfloat16)
    return (mixed_state, hidden_second)


def solution(mesh):
    in_specs = (
        P(("grp", "fs", "tp"), None),
        P(("grp", "fs", "tp"), None),
        P("tp", "fs"),
        P(("grp", "fs", "tp"), None),
        P(),
        P(),
        P("fs", "tp"),
        P("fs", "tp"),
    )
    out_specs = (P(("grp", "fs", "tp"), None), P(("grp", "fs"), "tp"))
    return jax.shard_map(
        on_device, mesh=mesh, in_specs=in_specs, out_specs=out_specs, check_vma=False
    )
```

profile of v0, /device:TPU:0, one launch (start us, length us, event | category | flops | bytes accessed | tf_op | source)
XLA Modules:
  0.0 405.8 jit_solution(10597806756419352990)
XLA Ops:
  7.2 0.0 all-gather.4.cloned.1.call-start
  7.2 0.7 all-gather.4.cloned.1.call-update
  7.9 0.0 reduce-scatter.2.cloned.1.call-start
  7.9 1.8 copy.10
  9.8 22.7 %all_to_all.19 = bf16[128,4,1408]{0,2,1:T(8,128)(2,1)S(1)} all-to-all(bf16[128,4,1408]{0,2,1:T(8,128)(2,1)S(1)} %bitcast.12), channel_id=1, replica_groups=mesh['grp'=2,'fs'=4,'tp'=4] {'tp'}, dimensions={1} | all-to-all | bytes 2883584 | tf_op jit(solution)/shard_map/all_to_all | solution.py:16
  32.5 0.8 copy.11
  33.3 85.7 %all-gather.4.cloned.1.call-done = bf16[1408,2048]{1,0:T(8,128)(2,1)} async-done(((bf16[1408,512]{1,0:T(8,128)(2,1)}), bf16[1408,2048]{1,0:T(8,128)(2,1)}) %all-gather.4.cloned.1.call-update) | async-done | bytes 5767184 | tf_op jit(solution)/shard_map/all_gather | solution.py:17
  119.0 0.0 copy-start.3
  119.0 0.0 copy-start.4
  119.0 0.0 copy-start
  119.0 7.2 %convolution_convert_fusion = bf16[512,2048]{1,0:T(8,128)(2,1)} fusion(bf16[512,1408]{1,0:T(8,128)(2,1)S(1)} %bitcast.13, bf16[1408,2048]{1,0:T(8,128)(2,1)} %all-gather.4.cloned.1.call-done), kind=kOutput, calls=%fused_computation | convolution fusion | flops 2953838592 | bytes 9306112 | tf_op jit(solution)/shard_map/dot_general | solution.py:19
  126.2 0.0 reduce-scatter.2.cloned.1.call-update
  126.3 0.0 all-gather.6.cloned.1.call-start
  126.3 0.0 copy-done.3
  126.3 0.0 copy-done.4
  126.4 29.5 %reduce-scatter.2.cloned.1.call-done = bf16[128,2048]{1,0:T(8,128)(2,1)} async-done(((bf16[512,2048]{1,0:T(8,128)(2,1)}), bf16[128,2048]{1,0:T(8,128)(2,1)}) %reduce-scatter.2.cloned.1.call-update) | async-done | bytes 524304 | tf_op jit(solution)/shard_map/reduce_scatter | solution.py:18
  155.9 0.0 copy-done
  155.9 1.3 fusion.1
  157.2 1.4 multiply_reduce_fusion.1
  158.6 0.0 copy-start.1
  158.6 0.0 copy-start.2
  158.6 1.9 fusion.2
  160.5 0.3 multiply_reduce_fusion
  160.8 1.1 add_convert_fusion
  161.8 0.0 all-gather.6.cloned.1.call-update
  161.9 0.0 all-gather.8.cloned.1.call-start
  161.9 0.0 copy-done.1
  161.9 0.0 copy-done.2
  161.9 1.9 pad_maximum_fusion
  163.8 0.0 all-gather.8.cloned.1.call-update
  163.8 20.8 %all-gather.6.cloned.1.call-done = bf16[512,2048]{1,0:T(8,128)(2,1)} async-done(((bf16[128,2048]{1,0:T(8,128)(2,1)}), bf16[512,2048]{1,0:T(8,128)(2,1)}) %all-gather.6.cloned.1.call-update) | async-done | bytes 2097168 | tf_op jit(solution)/shard_map/all_gather | solution.py:30
  184.6 202.5 %all-gather.8.cloned.1.call-done = bf16[2048,2816]{1,0:T(8,128)(2,1)} async-done(((bf16[512,2816]{1,0:T(8,128)(2,1)}), bf16[2048,2816]{1,0:T(8,128)(2,1)}) %all-gather.8.cloned.1.call-update) | async-done | bytes 11534352 | tf_op jit(solution)/shard_map/all_gather | solution.py:35
  387.1 10.2 %fusion.5 = f32[512,2816]{1,0:T(8,128)S(1)} fusion(bf16[512,2048]{1,0:T(8,128)(2,1)} %all-gather.6.cloned.1.call-done, bf16[2048,2816]{1,0:T(8,128)(2,1)} %all-gather.8.cloned.1.call-done), kind=kOutput, calls=%fused_computation.17 | convolution fusion | flops 5905580032 | bytes 19398656 | tf_op jit(solution)/shard_map/dot_general | solution.py:33
  397.3 2.0 fusion
  (6 shorter events, 0.1 us)
Async XLA Ops:
  7.2 111.8 %all-gather.4.cloned.1.call-start = ((), (), s32[]{:S(2)}) async-start(), calls=%async_computation.2 | async-start | bytes 7208960 | tf_op jit(solution)/shard_map/all_gather | solution.py:17
  7.9 148.0 %reduce-scatter.2.cloned.1.call-start = ((), (), s32[]{:S(2)}) async-start(), calls=%async_computation.3 | async-start | bytes 2621440 | tf_op jit(solution)/shard_map/reduce_scatter | solution.py:18
  119.0 7.3 %copy-start.3 = (f32[2,2048]{1,0:T(2,128)S(1)}, f32[2,2048]{1,0:T(2,128)}, u32[]{:S(2)}) copy-start(f32[2,2048]{1,0:T(2,128)} %param.12) | copy-start | bytes 49156
  119.0 7.4 %copy-start.4 = (f32[2,2048]{1,0:T(2,128)S(1)}, f32[2,2048]{1,0:T(2,128)}, u32[]{:S(2)}) copy-start(f32[2,2048]{1,0:T(2,128)} %param.13) | copy-start | bytes 49156
  119.0 36.9 %copy-start = (bf16[128,2048]{1,0:T(8,128)(2,1)S(1)}, bf16[128,2048]{1,0:T(8,128)(2,1)}, u32[]{:S(2)}) copy-start(bf16[128,2048]{1,0:T(8,128)(2,1)} %param.8) | copy-start | bytes 1572868
  126.3 58.3 %all-gather.6.cloned.1.call-start = ((), (), s32[]{:S(2)}) async-start(), calls=%async_computation.4 | async-start | bytes 2621440 | tf_op jit(solution)/shard_map/all_gather | solution.py:30
  158.6 3.3 copy-start.1
  158.6 3.3 copy-start.2
  161.9 225.2 %all-gather.8.cloned.1.call-start = ((), (), s32[]{:S(2)}) async-start(), calls=%async_computation.5 | async-start | bytes 14417920 | tf_op jit(solution)/shard_map/all_gather | solution.py:35
Sparse Core Ops, SparseCore 0:
  9.5 109.3 all-gather.3
  126.4 29.4 reduce-scatter.1
  162.0 22.5 all-gather.5
  186.0 201.0 all-gather.7
where the time goes:
time: 406 us
  waiting for transfers between devices  339 us (83%)
  blocking collectives  22.7 us (6%)
  matrix products  17.4 us (4%)
  between operations  13.9 us (3%)
  other arithmetic  9.78 us (2%)
    all_gather x1, waiting for transfers between devices, on_device(): lax.all_gather(joined, 'fs', axis=0, tiled=True)  202 us
    all_gather x1, waiting for transfers between devices, on_device(): down_full = lax.all_gather(down_weight, 'fs', axis=1, tiled=True)  85.7 us
    reduce_scatter x1, waiting for transfers between devices, on_device(): lax.psum_scatter(jnp.dot(spread, down_full, preferred_element_type=jnp.fl...  29.5 us
    all_to_all x1, blocking collectives, on_device(): lax.all_to_all(hidden_first, 'tp', split_axis=1, concat_axis=0, tiled=True)  22.7 us
    all_gather x1, waiting for transfers between devices, on_device(): gathered = lax.all_gather(mixed_state, 'tp', axis=0, tiled=True)  20.8 us
    dot_general x1, matrix products, on_device(): jnp.dot(gathered, lax.all_gather(joined, 'fs', axis=0, tiled=True), prefe...  10.2 us
  transfers between devices with their start and end apart: 4, of which 4 were waited for; matrix products, arithmetic and copies ran while one was open for 1% of the time, Pallas kernels for 0%

commit v1 on v0

v1 whole, which is shorter than its diff:
```python
import functools

import jax
import jax.numpy as jnp
from jax import lax
from jax.experimental import pallas as pl
from jax.experimental.pallas import tpu as pltpu
from jax.sharding import PartitionSpec as P

MESH = pl.DeviceIdType.MESH


def layer_norm(values, gain, shift):
    center = values - jnp.mean(values, axis=-1, keepdims=True)
    variance = jnp.mean(center * center, axis=-1, keepdims=True)
    return center * lax.rsqrt(variance + 1e-05) * gain + shift


def kernel(
    sizes,
    res_ref,
    hid_ref,
    down_ref,
    mix_ref,
    gain_ref,
    shift_ref,
    gate_ref,
    up_ref,
    mixed_ref,
    out_ref,
    down_all,
    pair_all,
    spread,
    part,
    red,
    mixed_all,
    acc,
    load_sem,
    d_send,
    d_recv,
    w_send,
    w_recv,
    a_send,
    a_recv,
    r_send,
    r_recv,
    m_send,
    m_recv,
):
    n_grp, n_fs, n_tp, sub = sizes
    g, f, t = lax.axis_index("grp"), lax.axis_index("fs"), lax.axis_index("tp")
    rows = res_ref.shape[0]
    width = gate_ref.shape[1]
    depth = gate_ref.shape[0]
    cols = down_ref.shape[1]
    chunks = n_grp * sub
    d_rows = down_ref.shape[0] // chunks
    w_rows = depth // chunks

    def hid_block(peer):
        if len(hid_ref.shape) == 3:
            return hid_ref.at[peer]
        return hid_ref.at[:, pl.ds(pl.multiple_of(peer * width, width), width)]

    def own_rows(peer):
        return pl.ds(pl.multiple_of(peer * rows, rows), rows)

    load_down = pltpu.make_async_copy(down_ref, down_all.at[f], load_sem.at[0])
    load_gate = pltpu.make_async_copy(gate_ref, pair_all.at[f, 0], load_sem.at[1])
    load_up = pltpu.make_async_copy(up_ref, pair_all.at[f, 1], load_sem.at[2])
    load_hid = pltpu.make_async_copy(hid_block(t), spread.at[own_rows(t)], load_sem.at[3])
    load_down.start()
    load_hid.start()
    load_gate.start()
    load_up.start()

    barrier = pltpu.get_barrier_semaphore()

    def greet(device):
        pl.semaphore_signal(barrier, inc=1, device_id=device, device_id_type=MESH)

    for d in range(1, n_grp):
        greet({"grp": lax.rem(g + d, n_grp)})
    for d in range(1, n_tp):
        greet({"tp": lax.rem(t + d, n_tp)})

    @pl.when(f > 0)
    def _():
        greet({"fs": f - 1})

    @pl.when(f < n_fs - 1)
    def _():
        greet({"fs": f + 1})

    inner = jnp.minimum(f, 1) + jnp.minimum(n_fs - 1 - f, 1)
    pl.semaphore_wait(barrier, n_grp - 1 + n_tp - 1 + inner)

    def d_copy(src, chunk, way, device):
        block = down_all.at[src, pl.ds(pl.multiple_of(chunk * d_rows, d_rows), d_rows)]
        return pltpu.make_async_remote_copy(
            src_ref=block,
            dst_ref=block,
            send_sem=d_send.at[way, src, chunk],
            recv_sem=d_recv.at[src, chunk],
            device_id=device,
            device_id_type=MESH,
        )

    def w_copy(mat):
        def copy(src, chunk, way, device):
            block = pair_all.at[src, mat, pl.ds(pl.multiple_of(chunk * w_rows, w_rows), w_rows)]
            return pltpu.make_async_remote_copy(
                src_ref=block,
                dst_ref=block,
                send_sem=w_send.at[way, 2 * src + mat, chunk],
                recv_sem=w_recv.at[2 * src + mat, chunk],
                device_id=device,
                device_id_type=MESH,
            )

        return copy

    def along(copy, src, chunk, act):
        @pl.when((f < n_fs - 1) & (src <= f))
        def _():
            act(copy(src, chunk, 0, {"fs": f + 1}))

        @pl.when((f > 0) & (src >= f))
        def _():
            act(copy(src, chunk, 1, {"fs": f - 1}))

    def across(copy, src, chunk, act):
        for d in range(1, n_grp):
            act(copy(src, chunk, 1 + d, {"grp": lax.rem(g + d, n_grp)}))

    def start(copy):
        copy.start()

    def wait_send(copy):
        copy.wait_send()

    def take(copies, src):
        for j in range(sub):
            for copy in copies:
                chunk = g * sub + j
                copy(src, chunk, 0, {"fs": f}).wait_recv()
                along(copy, src, chunk, start)
                across(copy, src, chunk, start)

    def take_across(copies, src):
        for d in range(1, n_grp):
            peer = lax.rem(g + d, n_grp)
            for j in range(sub):
                for copy in copies:
                    copy(src, peer * sub + j, 0, {"fs": f}).wait_recv()

    def source(k):
        return f + (1 - 2 * lax.rem(k, 2)) * ((k + 1) // 2)

    def valid(src):
        return (src >= 0) & (src < n_fs)

    w_copies = [w_copy(0), w_copy(1)]

    def a_copy(d):
        peer = lax.rem(t + d, n_tp)
        return pltpu.make_async_remote_copy(
            src_ref=hid_block(peer),
            dst_ref=spread.at[own_rows(t)],
            send_sem=a_send.at[d],
            recv_sem=a_recv.at[d],
            device_id={"tp": peer},
            device_id_type=MESH,
        )

    def r_copy(src, d):
        peer = lax.rem(t + d, n_tp)
        return pltpu.make_async_remote_copy(
            src_ref=part.at[src, own_rows(peer)],
            dst_ref=red.at[d, src],
            send_sem=r_send.at[d, src],
            recv_sem=r_recv.at[d, src],
            device_id={"tp": peer},
            device_id_type=MESH,
        )

    def m_copy(d):
        peer = lax.rem(t + d, n_tp)
        return pltpu.make_async_remote_copy(
            src_ref=mixed_all.at[own_rows(t)],
            dst_ref=mixed_all.at[own_rows(t)],
            send_sem=m_send.at[d],
            recv_sem=m_recv.at[d],
            device_id={"tp": peer},
            device_id_type=MESH,
        )

    load_down.wait()
    for j in range(sub):
        along(d_copy, f, g * sub + j, start)
    for d in range(1, n_tp):
        a_copy(d).start()
    load_gate.wait()
    load_up.wait()
    load_hid.wait()

    def first_half(k, carry):
        src = source(k)

        @pl.when(valid(src))
        def _():
            take([d_copy], src)

        @pl.when(k == 2 * n_fs - 2)
        def _():
            for j in range(sub):
                for copy in w_copies:
                    along(copy, f, g * sub + j, start)

        @pl.when(k == 2)
        def _():
            for d in range(1, n_tp):
                a_copy(d).wait_recv()

        done = source(k - 2)

        @pl.when((k >= 2) & valid(done))
        def _():
            @pl.when(k > 2)
            def _():
                take_across([d_copy], done)

            part[done] = jnp.dot(
                spread[...], down_all[done], preferred_element_type=jnp.float32
            ).astype(jnp.bfloat16)
            for d in range(1, n_tp):
                r_copy(done, d).start()

        return carry

    lax.fori_loop(1, 2 * n_fs + 1, first_half, 0)

    for src in range(n_fs):
        for d in range(1, n_tp):
            r_copy(src, d).wait_recv()
    pieces = []
    for src in range(n_fs):
        total = part[src, own_rows(t)].astype(jnp.float32)
        for d in range(1, n_tp):
            total = total + red[d, src].astype(jnp.float32)
        pieces.append(total)
    branch = jnp.concatenate(pieces, axis=1)
    first = layer_norm(
        jnp.sqrt(2.0) * res_ref[...].astype(jnp.float32) + 0.5 * branch,
        gain_ref[0:1],
        shift_ref[0:1],
    )
    mixed = layer_norm(
        jnp.sqrt(2.0) * first + mix_ref[...].astype(jnp.float32), gain_ref[1:2], shift_ref[1:2]
    ).astype(jnp.bfloat16)
    mixed_all[own_rows(t)] = mixed
    mixed_ref[...] = mixed
    for d in range(1, n_tp):
        m_copy(d).start()
    acc[...] = jnp.zeros_like(acc)

    def second_half(k, carry):
        src = source(k)

        @pl.when(valid(src))
        def _():
            take(w_copies, src)

        @pl.when(k == 2)
        def _():
            for d in range(1, n_tp):
                m_copy(d).wait_recv()

        done = source(k - 2)

        @pl.when((k >= 2) & valid(done))
        def _():
            @pl.when(k > 2)
            def _():
                take_across(w_copies, done)

            here = pl.ds(pl.multiple_of(done * depth, depth), depth)
            for mat in range(2):
                acc[mat] += jnp.dot(
                    mixed_all[:, here], pair_all[done, mat], preferred_element_type=jnp.float32
                )

        return carry

    lax.fori_loop(1, 2 * n_fs + 1, second_half, 0)
    gate = acc[0]
    out_ref[...] = (gate / (1.0 + jnp.exp(-gate)) * acc[1]).astype(jnp.bfloat16)

    for d in range(1, n_tp):
        a_copy(d).wait_send()
        m_copy(d).wait_send()
        for src in range(n_fs):
            r_copy(src, d).wait_send()

    def drain(src, carry):
        for copy in [d_copy] + w_copies:
            for j in range(sub):
                along(copy, src, g * sub + j, wait_send)

                @pl.when(src != f)
                def _():
                    across(copy, src, g * sub + j, wait_send)

        return carry

    lax.fori_loop(0, n_fs, drain, 0)


def on_device(
    sizes,
    residual_in,
    hidden_first,
    down_weight,
    mixer_out,
    norm_gain,
    norm_shift,
    gate_weight,
    up_weight,
):
    n_grp, n_fs, n_tp = sizes
    rows, model = residual_in.shape
    depth, width = gate_weight.shape
    cols = down_weight.shape[1]
    sub = 1
    if depth % (n_grp * 2 * 32) == 0 and down_weight.shape[0] % (n_grp * 2 * 32) == 0:
        sub = 2
    chunks = n_grp * sub
    if width % 128:
        hidden_first = hidden_first.reshape(rows, n_tp, width).transpose(1, 0, 2)
    vmem = pl.BlockSpec(memory_space=pltpu.VMEM)
    anywhere = pl.BlockSpec(memory_space=pl.ANY)
    dma = pltpu.SemaphoreType.DMA
    tokens = rows * n_tp
    return pl.pallas_call(
        functools.partial(kernel, (n_grp, n_fs, n_tp, sub)),
        out_shape=(
            jax.ShapeDtypeStruct((rows, model), jnp.bfloat16),
            jax.ShapeDtypeStruct((tokens, width), jnp.bfloat16),
        ),
        in_specs=[vmem, anywhere, anywhere, vmem, vmem, vmem, anywhere, anywhere],
        out_specs=(vmem, vmem),
        scratch_shapes=[
            pltpu.VMEM((n_fs,) + down_weight.shape, jnp.bfloat16),
            pltpu.VMEM((n_fs, 2, depth, width), jnp.bfloat16),
            pltpu.VMEM((tokens, width), jnp.bfloat16),
            pltpu.VMEM((n_fs, tokens, cols), jnp.bfloat16),
            pltpu.VMEM((n_tp, n_fs, rows, cols), jnp.bfloat16),
            pltpu.VMEM((tokens, model), jnp.bfloat16),
            pltpu.VMEM((2, tokens, width), jnp.float32),
            dma((4,)),
            dma((1 + n_grp, n_fs, chunks)),
            dma((n_fs, chunks)),
            dma((1 + n_grp, 2 * n_fs, chunks)),
            dma((2 * n_fs, chunks)),
            dma((n_tp,)),
            dma((n_tp,)),
            dma((n_tp, n_fs)),
            dma((n_tp, n_fs)),
            dma((n_tp,)),
            dma((n_tp,)),
        ],
        compiler_params=pltpu.CompilerParams(
            collective_id=0, has_side_effects=True, vmem_limit_bytes=60 * 1024 * 1024
        ),
        name="half_steps",
    )(
        residual_in,
        hidden_first,
        down_weight,
        mixer_out,
        norm_gain,
        norm_shift,
        gate_weight,
        up_weight,
    )


def solution(mesh):
    sizes = tuple(mesh.shape[axis] for axis in ("grp", "fs", "tp"))
    in_specs = (
        P(("grp", "fs", "tp"), None),
        P(("grp", "fs", "tp"), None),
        P("tp", "fs"),
        P(("grp", "fs", "tp"), None),
        P(),
        P(),
        P("fs", "tp"),
        P("fs", "tp"),
    )
    out_specs = (P(("grp", "fs", "tp"), None), P(("grp", "fs"), "tp"))
    return jax.shard_map(
        functools.partial(on_device, sizes),
        mesh=mesh,
        in_specs=in_specs,
        out_specs=out_specs,
        check_vma=False,
    )
```

time: 406 us -> 174 us (0.43)
  waiting for transfers between devices: 339 us -> 0 us
  Pallas kernels: 0 us -> 169 us
  blocking collectives: 22.7 us -> 0 us
  matrix products: 17.4 us -> 0 us
  between operations: 13.9 us -> 0.64 us
  other arithmetic: 9.78 us -> 0 us
    all_gather x3 -> x0, waiting for transfers between devices: 309 us -> none  [the longest x1 202 us: on_device(): lax.all_gather(joined, 'fs', axis=0, tiled=True)]
    pallas_call x0 -> x1, Pallas kernels: none -> 169 us  [on_device(): pl.pallas_call(functools.partial(kernel, (n_grp, n_fs, n_tp, sub)), out_s...]
    reduce_scatter x1 -> x0, waiting for transfers between devices: 29.5 us -> none  [on_device(): lax.psum_scatter(jnp.dot(spread, down_full, preferred_element_type=jnp.fl...]
    all_to_all x1 -> x0, blocking collectives: 22.7 us -> none  [on_device(): lax.all_to_all(hidden_first, 'tp', split_axis=1, concat_axis=0, tiled=True)]
    dot_general x2 -> x0, matrix products: 17.4 us -> none  [the longest x1 10.2 us: on_device(): jnp.dot(gathered, lax.all_gather(joined, 'fs', axis=0, tiled=True), prefe...]
    reduce_sum x4 -> x0, other arithmetic: 4.88 us -> none  [the longest x2 3.22 us: layer_norm(): center = values - jnp.mean(values, axis=-1, keepdims=True)]
  transfers between devices with their start and end apart: 4 -> 0, of which waited for: 4 -> 0; matrix products, arithmetic and copies ran while one was open for 1% -> 0% of each run, Pallas kernels for 0% -> 0%
where the time goes in v1:
time: 174 us
  Pallas kernels  169 us (97%)
  local copies, waits for them, and re-layouts  4.45 us (3%)
    pallas_call x1, Pallas kernels, on_device(): pl.pallas_call(functools.partial(kernel, (n_grp, n_fs, n_tp, sub)), out_s...  169 us
    unnamed x2, local copies, waits for them, and re-layouts  4.45 us

profile of v1, /device:TPU:0, one launch (start us, length us, event | category | flops | bytes accessed | tf_op | source)
XLA Modules:
  0.0 174.0 jit_solution(7508399024632489135)
XLA Ops:
  0.6 168.9 %half_steps.1 = (bf16[128,2048]{1,0:T(8,128)(2,1)}, bf16[512,1408]{1,0:T(8,128)(2,1)}) custom-call(bf16[128,2048]{1,0:T(8,128)(2,1)} %res_ref.1, bf16[128,5632]{1,0:T(8,128)(2,1)} %hid_ref.1, bf16[1408,512]{1,0:T(8,128)(2,1)} %down_ref.1, bf16[128,2048]{1,0:T(8,128)(2,1)} %mix_ref.1, f32[2,2048]{1,0:T(2,128)} %gain_ref.1, f32[2,2048]{1,0:T(2,128)} %shift_ref.1, ...), custom_call_target="tpu_custom_call" | custom-call | tf_op jit(solution)/shard_map/half_steps/pallas_call | solution.py:344
  169.6 1.9 %copy.12 = bf16[128,2048]{1,0:T(8,128)(2,1)} copy(bf16[128,2048]{1,0:T(8,128)(2,1)} %get-tuple-element.4) | data formatting | bytes 1048576
  171.4 2.6 %copy.13 = bf16[512,1408]{1,0:T(8,128)(2,1)} copy(bf16[512,1408]{1,0:T(8,128)(2,1)} %get-tuple-element.5) | data formatting | bytes 2883584

commit v2 on v1

v2 whole, which is shorter than its diff:
```python
import functools

import jax
import jax.numpy as jnp
from jax import lax
from jax.experimental import pallas as pl
from jax.experimental.pallas import tpu as pltpu
from jax.sharding import PartitionSpec as P

MESH = pl.DeviceIdType.MESH


def layer_norm(values, gain, shift):
    center = values - jnp.mean(values, axis=-1, keepdims=True)
    variance = jnp.mean(center * center, axis=-1, keepdims=True)
    return center * lax.rsqrt(variance + 1e-05) * gain + shift


def kernel(
    sizes,
    res_ref,
    hid_ref,
    down_ref,
    mix_ref,
    gain_ref,
    shift_ref,
    gate_ref,
    up_ref,
    mixed_ref,
    out_ref,
    down_all,
    host_all,
    each_all,
    spread,
    part,
    red,
    mixed_all,
    host_acc,
    each_acc,
    back,
    load_sem,
    d_send,
    d_recv,
    h_send,
    h_recv,
    e_send,
    e_recv,
    a_send,
    a_recv,
    r_send,
    r_recv,
    m_send,
    m_recv,
    g_send,
    g_recv,
    b_send,
    b_recv,
):
    n_grp, n_fs, n_tp, sub = sizes
    shared = host_all.shape[3]
    g, f, t = lax.axis_index("grp"), lax.axis_index("fs"), lax.axis_index("tp")
    rows = res_ref.shape[0]
    width = gate_ref.shape[1]
    depth = gate_ref.shape[0]
    chunks = n_grp * sub

    def hid_block(peer):
        if len(hid_ref.shape) == 3:
            return hid_ref.at[peer]
        return hid_ref.at[:, pl.ds(pl.multiple_of(peer * width, width), width)]

    def own_rows(peer):
        return pl.ds(pl.multiple_of(peer * rows, rows), rows)

    load_down = pltpu.make_async_copy(down_ref, down_all.at[f], load_sem.at[0])
    loads = []
    for mat, ref in enumerate((gate_ref, up_ref)):
        loads.append(
            pltpu.make_async_copy(
                ref.at[:, pl.ds(0, shared)], host_all.at[f, mat], load_sem.at[1 + mat]
            )
        )
        loads.append(
            pltpu.make_async_copy(
                ref.at[:, pl.ds(shared, width - shared)], each_all.at[f, mat], load_sem.at[4 + mat]
            )
        )
    load_hid = pltpu.make_async_copy(hid_block(t), spread.at[own_rows(t)], load_sem.at[3])
    load_down.start()
    load_hid.start()
    for load in loads:
        load.start()

    lower = 2 * (f // 2)
    half = n_fs // 2
    host = lower + jnp.where(lower + 1 < half, 1, 0)
    is_host = f == host
    other = 2 * lower + 1 - f
    low_host = 1 if half > 1 else 0
    high_host = 2 * ((n_fs - 1) // 2)

    barrier = pltpu.get_barrier_semaphore()

    def greet(device):
        pl.semaphore_signal(barrier, inc=1, device_id=device, device_id_type=MESH)

    for d in range(1, n_grp):
        greet({"grp": lax.rem(g + d, n_grp)})
    for d in range(1, n_tp):
        greet({"tp": lax.rem(t + d, n_tp)})

    @pl.when(f > 0)
    def _():
        greet({"fs": f - 1})

    @pl.when(f < n_fs - 1)
    def _():
        greet({"fs": f + 1})

    inner = jnp.minimum(f, 1) + jnp.minimum(n_fs - 1 - f, 1)
    pl.semaphore_wait(barrier, n_grp - 1 + n_tp - 1 + inner)

    def block_copy(all_refs, send, recv):
        def copy(src, chunk, way, device):
            blocks = all_refs(src)
            size = blocks.shape[0] // chunks
            block = blocks.at[pl.ds(pl.multiple_of(chunk * size, size), size)]
            return pltpu.make_async_remote_copy(
                src_ref=block,
                dst_ref=block,
                send_sem=send(src).at[way, chunk],
                recv_sem=recv(src).at[chunk],
                device_id=device,
                device_id_type=MESH,
            )

        return copy

    def weight(refs, send, recv, mat):
        return block_copy(
            lambda src: refs.at[src, mat],
            lambda src: send.at[2 * src + mat],
            lambda src: recv.at[2 * src + mat],
        )

    def start(copy):
        copy.start()

    def wait_send(copy):
        copy.wait_send()

    class Gather:
        def __init__(self, copies, low, high, whole, needs):
            self.copies, self.low, self.high = copies, low, high
            self.whole, self.needs = whole, needs

        def whole_up(self, plane):
            return (2 * plane < n_fs) & self.whole

        def whole_down(self, plane):
            return (2 * plane >= n_fs) & self.whole

        def reached(self, plane):
            return (plane >= self.low) & (plane <= self.high)

        def along(self, copy, src, chunk, act, mine):
            up = (src <= f) & self.reached(f + 1)
            down = (src >= f) & self.reached(f - 1)
            if not mine:
                up = up & self.whole_up(f + 1)
                down = down & self.whole_down(f - 1)

            @pl.when(up)
            def _():
                act(copy(src, chunk, 0, {"fs": f + 1}))

            @pl.when(down)
            def _():
                act(copy(src, chunk, 1, {"fs": f - 1}))

        def all_along(self, src, act):
            for j in range(sub):
                for copy in self.copies:
                    self.along(copy, src, g * sub + j, act, True)
            if self.whole:
                for d in range(1, n_grp):
                    for j in range(sub):
                        for copy in self.copies:
                            chunk = lax.rem(g + d, n_grp) * sub + j
                            self.along(copy, src, chunk, act, False)

        def across(self, copy, src, chunk, act):
            for d in range(1, n_grp):
                act(copy(src, chunk, 1 + d, {"grp": lax.rem(g + d, n_grp)}))

        def whole_in(self, src):
            return ((src < f) & self.whole_up(f)) | ((src > f) & self.whole_down(f))

        def comes(self, src):
            return (src >= 0) & (src < n_fs) & (src != f) & self.reached(f)

        def swaps(self, src):
            return self.comes(src) & self.needs & jnp.logical_not(self.whole_in(src))

        def take(self, src):
            @pl.when(self.comes(src))
            def _():
                for j in range(sub):
                    for copy in self.copies:
                        chunk = g * sub + j
                        copy(src, chunk, 0, {"fs": other}).wait_recv()
                        self.along(copy, src, chunk, start, True)

                        @pl.when(self.swaps(src))
                        def _():
                            self.across(copy, src, chunk, start)

            if self.whole:

                @pl.when(self.comes(src) & self.whole_in(src))
                def _():
                    for d in range(1, n_grp):
                        for j in range(sub):
                            for copy in self.copies:
                                chunk = lax.rem(g + d, n_grp) * sub + j
                                copy(src, chunk, 0, {"fs": other}).wait_recv()
                                self.along(copy, src, chunk, start, False)

        def take_across(self, src):
            @pl.when(self.swaps(src))
            def _():
                for d in range(1, n_grp):
                    for j in range(sub):
                        for copy in self.copies:
                            chunk = lax.rem(g + d, n_grp) * sub + j
                            copy(src, chunk, 0, {"fs": other}).wait_recv()

        def drain(self, src):
            @pl.when((src == f) | self.comes(src))
            def _():
                if self.whole:
                    @pl.when((src == f) | self.whole_in(src))
                    def _():
                        for d in range(1, n_grp):
                            for j in range(sub):
                                for copy in self.copies:
                                    chunk = lax.rem(g + d, n_grp) * sub + j
                                    self.along(copy, src, chunk, wait_send, False)
                for j in range(sub):
                    for copy in self.copies:
                        self.along(copy, src, g * sub + j, wait_send, True)

            @pl.when(self.swaps(src))
            def _():
                for j in range(sub):
                    for copy in self.copies:
                        self.across(copy, src, g * sub + j, wait_send)

    def source(k):
        return f + (1 - 2 * lax.rem(k, 2)) * ((k + 1) // 2)

    def valid(src):
        return (src >= 0) & (src < n_fs)

    d_copy = block_copy(
        lambda src: down_all.at[src], lambda src: d_send.at[src], lambda src: d_recv.at[src]
    )
    down = Gather([d_copy], 0, n_fs - 1, False, True)
    hosted = Gather(
        [weight(host_all, h_send, h_recv, mat) for mat in range(2)],
        low_host,
        high_host,
        True,
        is_host,
    )
    each = Gather(
        [weight(each_all, e_send, e_recv, mat) for mat in range(2)], 0, n_fs - 1, True, True
    )

    def a_copy(d):
        peer = lax.rem(t + d, n_tp)
        return pltpu.make_async_remote_copy(
            src_ref=hid_block(peer),
            dst_ref=spread.at[own_rows(t)],
            send_sem=a_send.at[d],
            recv_sem=a_recv.at[d],
            device_id={"tp": peer},
            device_id_type=MESH,
        )

    def r_copy(src, d):
        peer = lax.rem(t + d, n_tp)
        return pltpu.make_async_remote_copy(
            src_ref=part.at[src, own_rows(peer)],
            dst_ref=red.at[d, src],
            send_sem=r_send.at[d, src],
            recv_sem=r_recv.at[d, src],
            device_id={"tp": peer},
            device_id_type=MESH,
        )

    core = lax.rem(t, 2)
    sibling = t + 1 - 2 * core

    def m_copy(owner, whose, hop):
        peer = sibling if hop == 0 else lax.rem(t + 2 * hop, n_tp)
        place = mixed_all.at[whose, own_rows(owner)]
        return pltpu.make_async_remote_copy(
            src_ref=place,
            dst_ref=place,
            send_sem=m_send.at[whose, owner, hop],
            recv_sem=m_recv.at[whose, owner],
            device_id={"tp": peer},
            device_id_type=MESH,
        )

    chips = n_tp // 2

    def m_out(whose):
        for hop in list(range(1, chips)) + [0]:
            m_copy(t, whose, hop).start()

    def m_relay(whose):
        for hop in range(1, chips):
            owner = lax.rem(t + 2 * hop, n_tp)
            m_copy(owner, whose, 0).wait_recv()
            m_copy(owner, whose, 0).start()

    def m_rest(whose):
        for hop in range(chips):
            m_copy(lax.rem(sibling + 2 * hop, n_tp), whose, 0).wait_recv()

    def m_drain(whose):
        for hop in range(chips):
            m_copy(t, whose, hop).wait_send()
        for hop in range(1, chips):
            m_copy(lax.rem(t + 2 * hop, n_tp), whose, 0).wait_send()

    def g_copy():
        return pltpu.make_async_remote_copy(
            src_ref=mixed_all.at[0, own_rows(t)],
            dst_ref=mixed_all.at[1, own_rows(t)],
            send_sem=g_send.at[0],
            recv_sem=g_recv.at[0],
            device_id={"fs": other},
            device_id_type=MESH,
        )

    tiles = 2
    tile = n_tp * rows // tiles

    def tile_rows(i):
        return pl.ds(pl.multiple_of(i * tile, tile), tile)

    def b_copy(i):
        return pltpu.make_async_remote_copy(
            src_ref=back.at[tile_rows(i)],
            dst_ref=out_ref.at[tile_rows(i), pl.ds(0, shared)],
            send_sem=b_send.at[i],
            recv_sem=b_recv.at[i],
            device_id={"fs": other},
            device_id_type=MESH,
        )

    load_down.wait()
    down.all_along(f, start)
    for d in range(1, n_tp):
        a_copy(d).start()
    for load in loads:
        load.wait()
    load_hid.wait()

    @pl.when(jnp.logical_not(is_host))
    def _():
        hosted.all_along(f, start)

    def first_half(k, carry):
        src = source(k)

        down.take(src)

        @pl.when((k == 2 * n_fs - 2) & is_host)
        def _():
            hosted.all_along(f, start)

        @pl.when(k == 2)
        def _():
            for d in range(1, n_tp):
                a_copy(d).wait_recv()

        done = source(k - 2)

        @pl.when((k >= 2) & valid(done))
        def _():
            down.take_across(done)
            part[done] = jnp.dot(
                spread[...], down_all[done], preferred_element_type=jnp.float32
            ).astype(jnp.bfloat16)
            for d in range(1, n_tp):
                r_copy(done, d).start()

        return carry

    lax.fori_loop(1, 2 * n_fs + 1, first_half, 0)

    for src in range(n_fs):
        for d in range(1, n_tp):
            r_copy(src, d).wait_recv()
    pieces = []
    for src in range(n_fs):
        total = part[src, own_rows(t)].astype(jnp.float32)
        for d in range(1, n_tp):
            total = total + red[d, src].astype(jnp.float32)
        pieces.append(total)
    branch = jnp.concatenate(pieces, axis=1)
    first = layer_norm(
        jnp.sqrt(2.0) * res_ref[...].astype(jnp.float32) + 0.5 * branch,
        gain_ref[0:1],
        shift_ref[0:1],
    )
    mixed = layer_norm(
        jnp.sqrt(2.0) * first + mix_ref[...].astype(jnp.float32), gain_ref[1:2], shift_ref[1:2]
    ).astype(jnp.bfloat16)
    mixed_all[0, own_rows(t)] = mixed
    mixed_ref[...] = mixed

    @pl.when(jnp.logical_not(is_host))
    def _():
        g_copy().start()

    m_out(0)

    @pl.when(jnp.logical_not(is_host))
    def _():
        each.all_along(f, start)

    def take_hosted(k, carry):
        hosted.take(source(k))
        return carry

    lax.fori_loop(1, 2 * n_fs - 1, take_hosted, 0)

    @pl.when(is_host)
    def _():
        each.all_along(f, start)

    m_relay(0)

    @pl.when(is_host)
    def _():
        g_copy().wait_recv()
        m_out(1)

    def take_each(k, carry):
        each.take(source(k))
        return carry

    lax.fori_loop(1, 3, take_each, 0)
    m_rest(0)

    def products(whose, span, gather, refs, total):
        total[...] = jnp.zeros_like(total)

        def add(k, carry):
            src = source(k)

            @pl.when(valid(src))
            def _():
                if gather is not None:
                    gather.take_across(src)
                here = pl.ds(pl.multiple_of(src * depth, depth), depth)
                for mat in range(2):
                    total[mat] += jnp.dot(
                        mixed_all[whose, span, here],
                        refs[src, mat],
                        preferred_element_type=jnp.float32,
                    )

            return carry

        lax.fori_loop(0, 2 * n_fs - 1, add, 0)
        gate = total[0]
        return (gate / (1.0 + jnp.exp(-gate)) * total[1]).astype(jnp.bfloat16)

    everything = pl.ds(0, n_tp * rows)

    @pl.when(is_host)
    def _():
        m_relay(1)
        out_ref[:, pl.ds(0, shared)] = products(0, everything, hosted, host_all, host_acc)

    lax.fori_loop(3, 2 * n_fs - 1, take_each, 0)

    @pl.when(is_host)
    def _():
        m_rest(1)

        def serve(i, carry):
            back[tile_rows(i)] = products(
                1, tile_rows(i), None, host_all, host_acc.at[:, pl.ds(0, tile)]
            )
            b_copy(i).start()
            return carry

        lax.fori_loop(0, tiles, serve, 0)

    out_ref[:, pl.ds(shared, width - shared)] = products(0, everything, each, each_all, each_acc)

    @pl.when(is_host)
    def _():
        for i in range(tiles):
            b_copy(i).wait_send()
        m_drain(1)

    @pl.when(jnp.logical_not(is_host))
    def _():
        g_copy().wait_send()
        for i in range(tiles):
            b_copy(i).wait_recv()

    m_drain(0)
    for d in range(1, n_tp):
        a_copy(d).wait_send()
        for src in range(n_fs):
            r_copy(src, d).wait_send()

    def drain(src, carry):
        for gather in (down, hosted, each):
            gather.drain(src)
        return carry

    lax.fori_loop(0, n_fs, drain, 0)


def on_device(
    sizes,
    residual_in,
    hidden_first,
    down_weight,
    mixer_out,
    norm_gain,
    norm_shift,
    gate_weight,
    up_weight,
):
    n_grp, n_fs, n_tp = sizes
    rows, model = residual_in.shape
    depth, width = gate_weight.shape
    cols = down_weight.shape[1]
    sub = 1
    if depth % (n_grp * 2 * 32) == 0 and down_weight.shape[0] % (n_grp * 2 * 32) == 0:
        sub = 2
    chunks = n_grp * sub
    each = max(1, width * 3 // (11 * 128)) * 128
    shared = (width - each) // 128 * 128
    each = width - shared
    if width % 128:
        hidden_first = hidden_first.reshape(rows, n_tp, width).transpose(1, 0, 2)
    vmem = pl.BlockSpec(memory_space=pltpu.VMEM)
    anywhere = pl.BlockSpec(memory_space=pl.ANY)
    dma = pltpu.SemaphoreType.DMA
    tokens = rows * n_tp
    return pl.pallas_call(
        functools.partial(kernel, (n_grp, n_fs, n_tp, sub)),
        out_shape=(
            jax.ShapeDtypeStruct((rows, model), jnp.bfloat16),
            jax.ShapeDtypeStruct((tokens, width), jnp.bfloat16),
        ),
        in_specs=[vmem, anywhere, anywhere, vmem, vmem, vmem, anywhere, anywhere],
        out_specs=(vmem, vmem),
        scratch_shapes=[
            pltpu.VMEM((n_fs,) + down_weight.shape, jnp.bfloat16),
            pltpu.VMEM((n_fs, 2, depth, shared), jnp.bfloat16),
            pltpu.VMEM((n_fs, 2, depth, each), jnp.bfloat16),
            pltpu.VMEM((tokens, width), jnp.bfloat16),
            pltpu.VMEM((n_fs, tokens, cols), jnp.bfloat16),
            pltpu.VMEM((n_tp, n_fs, rows, cols), jnp.bfloat16),
            pltpu.VMEM((2, tokens, model), jnp.bfloat16),
            pltpu.VMEM((2, tokens, shared), jnp.float32),
            pltpu.VMEM((2, tokens, each), jnp.float32),
            pltpu.VMEM((tokens, shared), jnp.bfloat16),
            dma((6,)),
            dma((n_fs, 1 + n_grp, chunks)),
            dma((n_fs, chunks)),
            dma((2 * n_fs, 1 + n_grp, chunks)),
            dma((2 * n_fs, chunks)),
            dma((2 * n_fs, 1 + n_grp, chunks)),
            dma((2 * n_fs, chunks)),
            dma((n_tp,)),
            dma((n_tp,)),
            dma((n_tp, n_fs)),
            dma((n_tp, n_fs)),
            dma((2, n_tp, n_tp // 2)),
            dma((2, n_tp)),
            dma((1,)),
            dma((1,)),
            dma((2,)),
            dma((2,)),
        ],
        compiler_params=pltpu.CompilerParams(
            collective_id=0, has_side_effects=True, vmem_limit_bytes=60 * 1024 * 1024
        ),
        name="half_steps",
    )(
        residual_in,
        hidden_first,
        down_weight,
        mixer_out,
        norm_gain,
        norm_shift,
        gate_weight,
        up_weight,
    )


def solution(mesh):
    sizes = tuple(mesh.shape[axis] for axis in ("grp", "fs", "tp"))
    in_specs = (
        P(("grp", "fs", "tp"), None),
        P(("grp", "fs", "tp"), None),
        P("tp", "fs"),
        P(("grp", "fs", "tp"), None),
        P(),
        P(),
        P("fs", "tp"),
        P("fs", "tp"),
    )
    out_specs = (P(("grp", "fs", "tp"), None), P(("grp", "fs"), "tp"))
    return jax.shard_map(
        functools.partial(on_device, sizes),
        mesh=mesh,
        in_specs=in_specs,
        out_specs=out_specs,
        check_vma=False,
    )
```

time: 174 us -> 166 us (0.954)
  Pallas kernels: 169 us -> 161 us
    pallas_call x1, Pallas kernels: 169 us -> 161 us  [on_device(): pl.pallas_call(functools.partial(kernel, (n_grp, n_fs, n_tp, sub)), out_s...]
where the time goes in v2:
time: 166 us
  Pallas kernels  161 us (97%)
  local copies, waits for them, and re-layouts  4.45 us (3%)
    pallas_call x1, Pallas kernels, on_device(): pl.pallas_call(functools.partial(kernel, (n_grp, n_fs, n_tp, sub)), out_s...  161 us
    unnamed x2, local copies, waits for them, and re-layouts  4.45 us

profile of v2, /device:TPU:0, one launch (start us, length us, event | category | flops | bytes accessed | tf_op | source)
XLA Modules:
  0.0 166.2 jit_solution(10090212373627282068)
XLA Ops:
  0.6 161.1 %half_steps.1 = (bf16[128,2048]{1,0:T(8,128)(2,1)}, bf16[512,1408]{1,0:T(8,128)(2,1)}) custom-call(bf16[128,2048]{1,0:T(8,128)(2,1)} %res_ref.1, bf16[128,5632]{1,0:T(8,128)(2,1)} %hid_ref.1, bf16[1408,512]{1,0:T(8,128)(2,1)} %down_ref.1, bf16[128,2048]{1,0:T(8,128)(2,1)} %mix_ref.1, f32[2,2048]{1,0:T(2,128)} %gain_ref.1, f32[2,2048]{1,0:T(2,128)} %shift_ref.1, ...), custom_call_target="tpu_custom_call" | custom-call | tf_op jit(solution)/shard_map/half_steps/pallas_call | solution.py:563
  161.8 1.9 %copy.12 = bf16[128,2048]{1,0:T(8,128)(2,1)} copy(bf16[128,2048]{1,0:T(8,128)(2,1)} %get-tuple-element.4) | data formatting | bytes 1048576
  163.7 2.6 %copy.13 = bf16[512,1408]{1,0:T(8,128)(2,1)} copy(bf16[512,1408]{1,0:T(8,128)(2,1)} %get-tuple-element.5) | data formatting | bytes 2883584
